TPU v7x, 32 devices: a whole 2x2x4 slice. The times are simulated.
32 devices in a mesh: grp: 2 (over y), ep: 8 (over z, x), tp: 2 (over core).
Axes of the slice: x: 2, y: 2, z: 4, core: 2. Of those that a mesh axis runs over, the one named last changes fastest.
Arguments:
- tokens: bfloat16 [384, 2048], P(('grp', 'ep')), parts along dimension 0, may hold values from -6 to 6
- norm_gain: float32 [2048], replicated, may hold values from 0.1 to 1.9
- routes: int32 [384, 4], P(('grp', 'ep')), parts along dimension 0, may hold values from 0 to 7, all different within a row; in each aligned block of 24 rows (0 to 23, 24 to 47, ...) at most 24 rows name the same one
- gate_scores: float32 [384, 4], P(('grp', 'ep')), parts along dimension 0, may hold values from 0.05 to 1
- w_gate: bfloat16 [8, 2048, 512], P('ep', None, 'tp'), may hold values from -1 to 1
- w_up: bfloat16 [8, 2048, 512], P('ep', None, 'tp'), may hold values from -1 to 1
- w_down: bfloat16 [8, 512, 2048], P('ep', 'tp'), may hold values from -0.0625 to 0.0625
Outputs:
- mixed: bfloat16 [384, 2048], P(('grp', 'ep')), parts along dimension 0
There are 2 independent parts, one for each index of `grp`. A program takes and returns all parts, laid end to end along the dimension named above; an argument that names none is the same for every part. Nothing has to cross between parts.
Inputs may be any that keep to these rules, and one draw needn't show every extreme that they name: `routes`: each row names 4 different experts; among the 24 rows of one device no expert is named more than 24 times, a bound that some block reaches.
All inputs are finite; a program needn't handle non-finite values.
Results may differ from a plain program's by a relative error of at most 0.0077.
Values may be sent and summed in bfloat16 or wider, within the bound.
A program may use at most 64 MiB of HBM per device.

v0:
```python
import jax
import jax.numpy as jnp
from jax import lax
from jax.sharding import PartitionSpec as P


def clamped_unit(g, u):
    gate = jnp.minimum(g, 7.0)
    up = jnp.clip(u, -7.0, 7.0)
    return (up + 1.0) * gate * jax.nn.sigmoid(1.702 * gate)


def expert_rows(rows, wg, wu, wd):
    g = jnp.dot(rows, wg, preferred_element_type=jnp.float32)
    u = jnp.dot(rows, wu, preferred_element_type=jnp.float32)
    act = clamped_unit(g, u).astype(jnp.bfloat16)
    part = jnp.dot(act, wd, preferred_element_type=jnp.float32)
    part = lax.optimization_barrier(part.astype(jnp.bfloat16)).astype(jnp.float32)
    total = lax.psum(part.astype(jnp.bfloat16), "tp")
    return total


def finish(mixed):
    result = mixed.astype(jnp.bfloat16)
    return result


def slot_table(routes, scores, experts, capacity):
    count = routes.shape[0]
    chosen = routes[:, :, None] == experts[None, None, :]
    hit = jnp.any(chosen, axis=1).astype(jnp.int32)
    weight = jnp.sum(jnp.where(chosen, scores[:, :, None], 0.0), axis=1)
    rank = jnp.cumsum(hit, axis=0) - hit
    places = jnp.arange(capacity, dtype=jnp.int32)
    match = (hit[:, :, None] == 1) & (rank[:, :, None] == places[None, None, :])
    row_ids = jnp.arange(count, dtype=jnp.int32)[:, None, None]
    filled = jnp.any(match, axis=0)
    slot_tok = jnp.sum(jnp.where(match, row_ids, 0), axis=0) + count * (
        1 - filled.astype(jnp.int32)
    )
    slot_w = jnp.sum(jnp.where(match, weight[:, :, None], 0.0), axis=0)
    return (slot_tok, slot_w)


def body(tokens, norm_gain, routes, gate_scores, w_gate, w_up, w_down):
    count, width = tokens.shape
    top = routes.shape[1]
    nexp = lax.axis_size("ep")
    capacity = max(2, min(count, 2 * count * top // nexp))
    wg, wu, wd = (w_gate[0], w_up[0], w_down[0])
    xf = tokens.astype(jnp.float32)
    normed = (xf * lax.rsqrt(jnp.mean(xf * xf, axis=-1, keepdims=True) + 1e-06) * norm_gain).astype(
        jnp.bfloat16
    )
    experts = jnp.arange(nexp, dtype=jnp.int32)
    slot_tok, slot_w = slot_table(routes, gate_scores, experts, capacity)
    padded = jnp.concatenate([normed, jnp.zeros((1, width), jnp.bfloat16)], axis=0)
    outgoing = padded[slot_tok]
    received = lax.all_to_all(outgoing, "ep", split_axis=0, concat_axis=0, tiled=True)
    sources, places, _ = received.shape
    outputs = expert_rows(received.reshape(sources * places, width), wg, wu, wd)
    returned = lax.all_to_all(
        outputs.reshape(sources, places, outputs.shape[1]),
        "ep",
        split_axis=0,
        concat_axis=0,
        tiled=True,
    )
    flat_tok = slot_tok.reshape(-1)
    token_ids = jnp.arange(count, dtype=jnp.int32)
    combine = jnp.where(flat_tok[None, :] == token_ids[:, None], slot_w.reshape(-1)[None, :], 0.0)
    mixed = jnp.dot(
        combine,
        returned.reshape(-1, returned.shape[2]).astype(jnp.float32),
        precision=lax.Precision.HIGHEST,
    )
    return finish(mixed)


def solution(mesh):
    in_specs = (
        P(("grp", "ep"), None),
        P(),
        P(("grp", "ep"), None),
        P(("grp", "ep"), None),
        P("ep", None, "tp"),
        P("ep", None, "tp"),
        P("ep", "tp", None),
    )
    out_specs = P(("grp", "ep"), None)
    return jax.shard_map(body, mesh=mesh, in_specs=in_specs, out_specs=out_specs, check_vma=False)
```

profile of v0, /device:TPU:0, one launch (start us, length us, event | category | flops | bytes accessed | tf_op | source)
XLA Modules:
  0.0 94.1 jit_solution(17916535765891462060)
XLA Ops:
  6.5 0.0 copy-start
  6.5 0.0 all-reduce.3.cloned.1.call-start
  6.5 0.8 fusion.23
  7.3 0.1 copy.10
  7.5 0.1 fusion.21
  7.6 0.1 select_reduce_fusion.1
  7.7 1.0 %fusion.8 = f32[24]{0:T(128)S(1)} fusion(bf16[24,2048]{1,0:T(8,128)(2,1)} %param.7), kind=kLoop, calls=%fused_computation.14 | loop fusion | flops 147432 | bytes 98400 | tf_op jit(solution)/shard_map/reduce_sum | solution.py:52
  8.8 0.1 reshape.96
  8.9 1.0 %fusion.10 = bf16[24,2048]{1,0:T(8,128)(2,1)S(1)} fusion(bf16[24,2048]{1,0:T(8,128)(2,1)} %param.7, f32[2048]{0:T(1024)} %param.8, f32[24]{0:T(128)S(1)} %add_rsqrt_fusion), kind=kLoop, calls=%fused_computation.16 | loop fusion | flops 196608 | bytes 204896 | tf_op jit(solution)/shard_map/convert_element_type | solution.py:52
  9.9 1.1 %gather_fusion = bf16[192,2048]{1,0:T(8,128)(2,1)S(1)} fusion(bf16[25,2048]{1,0:T(8,128)(2,1)S(1)} %concatenate.3, s32[1024]{0:T(1024)S(1)} %pad_clamp_fusion), kind=kCustom, calls=%fused_computation | custom fusion | bytes 1573632 | tf_op jit(solution)/shard_map/gather | solution.py:58
  11.0 0.0 copy-start.1
  11.0 27.4 %all_to_all.10 = bf16[8,24,2048]{2,1,0:T(8,128)(2,1)S(1)} all-to-all(bf16[8,24,2048]{2,1,0:T(8,128)(2,1)S(1)} %bitcast.23), channel_id=1, replica_groups=mesh['grp'=2,'ep'=8,'tp'=2] {'ep'}, dimensions={0} | all-to-all | bytes 1572864 | tf_op jit(solution)/shard_map/all_to_all | solution.py:59
  38.4 0.0 copy-start.2
  38.4 0.0 copy-done.1
  38.4 0.4 convolution_minimum_fusion
  38.8 0.0 copy-done
  38.8 0.8 copy-done.2
  39.6 1.9 %convolution_convert_fusion = bf16[192,2048]{1,0:T(8,128)(2,1)} fusion(f32[192,256]{1,0:T(8,128)S(1)} %convolution_minimum_fusion, bf16[192,2048]{1,0:T(8,128)(2,1)S(1)} %bitcast.22, bf16[1,256,2048]{2,1,0:T(8,128)(2,1)S(1)} %copy-done, bf16[1,2048,256]{2,1,0:T(8,128)(2,1)S(1)} %copy-done.2), kind=kOutput, calls=%fused_computation.1 | convolution fusion | flops 403488768 | bytes 3866624 | tf_op jit(solution)/shard_map/dot_general | solution.py:17
  41.6 0.0 copy-start.3
  41.6 0.0 copy-start.4
  41.6 0.0 all-reduce.3.cloned.1.call-update
  41.6 18.2 %all-reduce.3.cloned.1.call-done = bf16[8,24,2048]{2,1,0:T(8,128)(2,1)} async-done(((bf16[8,24,2048]{2,1,0:T(8,128)(2,1)}), bf16[8,24,2048]{2,1,0:T(8,128)(2,1)}) %all-reduce.3.cloned.1.call-update) | async-done | bytes 786448 | tf_op jit(solution)/shard_map/psum | solution.py:19
  59.8 5.8 %all-to-all-start.1 = ((bf16[8,24,2048]{2,1,0:T(8,128)(2,1)}), bf16[8,24,2048]{2,1,0:T(8,128)(2,1)S(1)}, u32[]{:S(2)}, u32[]{:S(2)}) async-start(bf16[8,24,2048]{2,1,0:T(8,128)(2,1)} %all-reduce.3.cloned.1.call-done), calls=%async_computation.1 | async-start | bytes 1572864 | tf_op jit(solution)/shard_map/all_to_all | solution.py:62
  65.6 0.0 copy-done.3
  65.6 0.0 copy-done.4
  65.6 0.1 copy.11
  65.7 0.1 select_reduce_fusion
  65.8 0.1 broadcast_in_dim.69
  65.9 0.1 add.52
  66.0 20.2 %all-to-all-done.1 = bf16[8,24,2048]{2,1,0:T(8,128)(2,1)S(1)} async-done(((bf16[8,24,2048]{2,1,0:T(8,128)(2,1)}), bf16[8,24,2048]{2,1,0:T(8,128)(2,1)S(1)}, u32[]{:S(2)}, u32[]{:S(2)}) %all-to-all-start.1) | async-done | bytes 786464 | tf_op jit(solution)/shard_map/all_to_all | solution.py:62
  86.1 1.1 %convolution_convert_fusion.1 = bf16[24,2048]{1,0:T(8,128)(2,1)} fusion(bf16[192,2048]{1,0:T(8,128)(2,1)S(1)} %bitcast.24, f32[192]{0:T(256)S(1)} %broadcast_in_dim.69, s32[192]{0:T(256)S(1)} %add.52), kind=kOutput, calls=%fused_computation.2 | convolution fusion | flops 113304576 | bytes 886272 | tf_op jit(solution)/shard_map/dot_general | solution.py:72
  (8 shorter events, 0.1 us)
Async XLA Ops:
  6.5 32.3 %copy-start = (bf16[1,256,2048]{2,1,0:T(8,128)(2,1)S(1)}, bf16[1,256,2048]{2,1,0:T(8,128)(2,1)}, u32[]{:S(2)}) copy-start(bf16[1,256,2048]{2,1,0:T(8,128)(2,1)} %param.13) | copy-start | bytes 3145732
  6.5 53.2 %all-reduce.3.cloned.1.call-start = ((), (), s32[]{:S(2)}) async-start(), calls=%async_computation.2 | async-start | bytes 1572864 | tf_op jit(solution)/shard_map/psum | solution.py:19
  11.0 27.4 %copy-start.1 = (bf16[1,2048,256]{2,1,0:T(8,128)(2,1)S(1)}, bf16[1,2048,256]{2,1,0:T(8,128)(2,1)}, u32[]{:S(2)}) copy-start(bf16[1,2048,256]{2,1,0:T(8,128)(2,1)} %param.11) | copy-start | bytes 3145732
  38.4 1.2 %copy-start.2 = (bf16[1,2048,256]{2,1,0:T(8,128)(2,1)S(1)}, bf16[1,2048,256]{2,1,0:T(8,128)(2,1)}, u32[]{:S(2)}) copy-start(bf16[1,2048,256]{2,1,0:T(8,128)(2,1)} %param.12) | copy-start | bytes 3145732
  41.6 24.0 %copy-start.3 = (s32[24,4]{0,1:T(4,128)S(1)}, s32[24,4]{0,1:T(4,128)}, u32[]{:S(2)}) copy-start(s32[24,4]{0,1:T(4,128)} %param.9) | copy-start | bytes 1156
  41.6 24.0 %copy-start.4 = (f32[24,4]{0,1:T(4,128)S(1)}, f32[24,4]{0,1:T(4,128)}, u32[]{:S(2)}) copy-start(f32[24,4]{0,1:T(4,128)} %param.10) | copy-start | bytes 1156
  59.8 26.4 %all-to-all-start.1 = ((bf16[8,24,2048]{2,1,0:T(8,128)(2,1)}), bf16[8,24,2048]{2,1,0:T(8,128)(2,1)S(1)}, u32[]{:S(2)}, u32[]{:S(2)}) async-start(bf16[8,24,2048]{2,1,0:T(8,128)(2,1)} %all-reduce.3.cloned.1.call-done), calls=%async_computation.1 | async-start | bytes 1572864 | tf_op jit(solution)/shard_map/all_to_all | solution.py:62
Sparse Core Ops, SparseCore 0:
  41.7 17.9 all-reduce.2
where the time goes:
time: 94.4 us; the launch traced here: 94.1 us
  waiting for transfers between devices  38.3 us (41%)
  blocking collectives  27.4 us (29%)
  between operations  13.5 us (14%)
  starting transfers between devices  5.81 us (6%)
  matrix products  3.4 us (4%)
  other arithmetic  3.26 us (3%)
  local copies, waits for them, and re-layouts  2.39 us (3%)
    all_to_all x1, blocking collectives, body(): lax.all_to_all(outgoing, 'ep', split_axis=0, concat_axis=0, tiled=True)  27.4 us
    all_to_all x1, waiting for transfers between devices, body(): lax.all_to_all(outputs.reshape(sources, places, outputs.shape[1]), 'ep',...  20.2 us
    psum x1, waiting for transfers between devices, expert_rows(): total = lax.psum(part.astype(jnp.bfloat16), 'tp')  18.2 us
    all_to_all x1, starting transfers between devices, body(): lax.all_to_all(outputs.reshape(sources, places, outputs.shape[1]), 'ep',...  5.81 us
    dot_general x1, matrix products, expert_rows(): part = jnp.dot(act, wd, preferred_element_type=jnp.float32)  1.94 us
  transfers between devices with their start and end apart: 2, of which 2 were waited for; matrix products, arithmetic and copies ran while one was open for 0% of the time, Pallas kernels for 0%

commit v1 on v0

--- a/solution.py
+++ b/solution.py
@@ -1,7 +1,14 @@
+import functools
+
 import jax
 import jax.numpy as jnp
 from jax import lax
+from jax.experimental import pallas as pl
+from jax.experimental.pallas import tpu as pltpu
 from jax.sharding import PartitionSpec as P
+
+MESH = pl.DeviceIdType.MESH
+LANES = 128
 
 
 def clamped_unit(g, u):
@@ -42,7 +49,7 @@
     return (slot_tok, slot_w)
 
 
-def body(tokens, norm_gain, routes, gate_scores, w_gate, w_up, w_down):
+def exchange_body(tokens, norm_gain, routes, gate_scores, w_gate, w_up, w_down):
     count, width = tokens.shape
     top = routes.shape[1]
     nexp = lax.axis_size("ep")
@@ -77,6 +84,235 @@
     return finish(mixed)
 
 
+def moe_kernel(
+    nz,
+    tok_ref, gain_ref, routes_ref, score_ref, wg_hbm, wu_hbm, wd_hbm,
+    out_ref,
+    gath, wg, wu, wd, contrib, from_x, summed, from_z, res,
+    w_loc, w_send, w_recv, z_send, z_recv, x_send, x_recv,
+    rx_send, rx_recv, rz_send, rz_recv, f_send, f_recv,
+):
+    ep, tp = lax.axis_index("ep"), lax.axis_index("tp")
+    z, x = ep // 2, ep % 2
+    home = x == tp
+    count, width = tok_ref.shape
+
+    def at_z(zz):
+        return {"ep": zz * 2 + x, "tp": tp}
+
+    x_peer = {"ep": z * 2 + 1 - x, "tp": tp}
+    sibling = {"ep": ep, "tp": 1 - tp}
+    others = [(z + k) % nz for k in range(1, nz)]
+
+    barrier = pltpu.get_barrier_semaphore()
+    for zz in others:
+        pl.semaphore_signal(barrier, inc=1, device_id=at_z(zz), device_id_type=MESH)
+    pl.semaphore_signal(barrier, inc=1, device_id=x_peer, device_id_type=MESH)
+    pl.semaphore_signal(barrier, inc=1, device_id=sibling, device_id_type=MESH)
+
+    weights = ((wg_hbm, wg), (wu_hbm, wu), (wd_hbm, wd))
+    local = [
+        pltpu.make_async_copy(src.at[0], dst.at[tp], w_loc.at[i])
+        for i, (src, dst) in enumerate(weights)
+    ]
+    shared = [
+        pltpu.make_async_remote_copy(
+            src.at[0], dst.at[tp], w_send.at[i], w_recv.at[i], device_id=sibling, device_id_type=MESH
+        )
+        for i, (src, dst) in enumerate(weights)
+    ]
+    for c in local:
+        c.start()
+
+    @pl.when(home)
+    def _():
+        xf = tok_ref[...].astype(jnp.float32)
+        scale = lax.rsqrt(jnp.mean(xf * xf, axis=-1, keepdims=True) + 1e-06)
+        gath[z, :, :width] = (xf * scale * gain_ref[...]).astype(jnp.bfloat16)
+        lane = lax.broadcasted_iota(jnp.int32, (count, LANES), 1)
+        half = LANES // 2
+        expert = lane % half
+        w = jnp.zeros((count, LANES), jnp.float32)
+        for k in range(routes_ref.shape[1]):
+            w = w + jnp.where(routes_ref[:, k : k + 1] == expert, score_ref[:, k : k + 1], 0.0)
+        high = w.astype(jnp.bfloat16)
+        low = (w - high.astype(jnp.float32)).astype(jnp.bfloat16)
+        gath[z, :, width:] = jnp.where(
+            lane < half, high.astype(jnp.float32), low.astype(jnp.float32)
+        ).astype(jnp.bfloat16)
+
+    pl.semaphore_wait(barrier, nz + 1)
+    for c in shared:
+        c.start()
+
+    def along_z(zz, slot):
+        return pltpu.make_async_remote_copy(
+            gath.at[slot], gath.at[slot], z_send.at[zz], z_recv.at[slot],
+            device_id=at_z(zz), device_id_type=MESH,
+        )
+
+    def across_x(slot):
+        return pltpu.make_async_remote_copy(
+            gath.at[slot], gath.at[slot], x_send.at[slot], x_recv.at[slot],
+            device_id=x_peer, device_id_type=MESH,
+        )
+
+    order = [z] + [(z + k) % nz for k in ORDER if k < nz]
+
+    @pl.when(home)
+    def _():
+        for zz in order[1:]:
+            along_z(zz, z).start()
+        across_x(z).start()
+
+    def arrive(slot, own):
+        @pl.when(home)
+        def _():
+            if not own:
+                along_z(slot, slot).wait_recv()
+                across_x(slot).start()
+
+        @pl.when(jnp.logical_not(home))
+        def _():
+            across_x(slot).wait_recv()
+
+    def compute(slots):
+        rows = jnp.concatenate(
+            [gath[s, :, :width].astype(jnp.float32) for s in slots], axis=0
+        ).astype(jnp.bfloat16)
+        acts = []
+        for j in range(2):
+            g = jnp.dot(rows, wg[j], preferred_element_type=jnp.float32)
+            u = jnp.dot(rows, wu[j], preferred_element_type=jnp.float32)
+            gate = jnp.minimum(g, 7.0)
+            up = jnp.clip(u, -7.0, 7.0)
+            acts.append(((up + 1.0) * gate * jax.nn.sigmoid(1.702 * gate)).astype(jnp.bfloat16))
+        lane = lax.broadcasted_iota(jnp.int32, (count, LANES), 1)
+        mine = lane % (LANES // 2) == ep
+        weight = [
+            jnp.sum(
+                jnp.where(mine, gath[s, :, width:].astype(jnp.float32), 0.0), axis=1, keepdims=True
+            )
+            for s in slots
+        ]
+        step = width // 4
+        for c in range(0, width, step):
+            y = jnp.dot(acts[0], wd[0, :, c : c + step], preferred_element_type=jnp.float32)
+            y = y + jnp.dot(acts[1], wd[1, :, c : c + step], preferred_element_type=jnp.float32)
+            for i, s in enumerate(slots):
+                contrib[s, :, c : c + step] = (
+                    y[i * count : (i + 1) * count] * weight[i]
+                ).astype(jnp.bfloat16)
+
+    def back_x(slot):
+        return pltpu.make_async_remote_copy(
+            contrib.at[slot], from_x.at[slot], rx_send.at[slot], rx_recv.at[slot],
+            device_id=x_peer, device_id_type=MESH,
+        )
+
+    def back_z(zz, slot):
+        return pltpu.make_async_remote_copy(
+            summed.at[zz], from_z.at[slot], rz_send.at[zz], rz_recv.at[slot],
+            device_id=at_z(zz), device_id_type=MESH,
+        )
+
+    for i, slot in enumerate(order):
+        arrive(slot, i == 0)
+    for c in local:
+        c.wait()
+    for c in shared:
+        c.wait()
+    compute(order)
+
+    back = order[1:] + order[:1]
+
+    @pl.when(jnp.logical_not(home))
+    def _():
+        for slot in back:
+            back_x(slot).start()
+
+    final = pltpu.make_async_remote_copy(
+        res, res, f_send, f_recv, device_id=sibling, device_id_type=MESH
+    )
+
+    @pl.when(home)
+    def _():
+        for slot in back[:-1]:
+            back_x(slot).wait_recv()
+            summed[slot] = (
+                contrib[slot].astype(jnp.float32) + from_x[slot].astype(jnp.float32)
+            ).astype(jnp.bfloat16)
+            back_z(slot, z).start()
+        back_x(z).wait_recv()
+        total = contrib[z].astype(jnp.float32) + from_x[z].astype(jnp.float32)
+        for slot in back[:-1]:
+            back_z(slot, slot).wait_recv()
+            total = total + from_z[slot].astype(jnp.float32)
+        res[...] = total.astype(jnp.bfloat16)
+        final.start()
+        out_ref[...] = total.astype(out_ref.dtype)
+        for zz in order[1:]:
+            along_z(zz, z).wait_send()
+            back_z(zz, z).wait_send()
+        for slot in order:
+            across_x(slot).wait_send()
+        final.wait_send()
+
+    @pl.when(jnp.logical_not(home))
+    def _():
+        for slot in order:
+            back_x(slot).wait_send()
+        final.wait_recv()
+        out_ref[...] = res[...].astype(out_ref.dtype)
+
+
+ORDER = (1, 3, 2)
+
+
+def gather_body(tokens, norm_gain, routes, gate_scores, w_gate, w_up, w_down):
+    count, width = tokens.shape
+    nz = lax.axis_size("ep") // 2
+    hidden = w_gate.shape[2]
+    bf16 = jnp.bfloat16
+    dma = pltpu.SemaphoreType.DMA
+    block = (nz, count, width)
+    vmem = pl.BlockSpec(memory_space=pltpu.VMEM)
+    hbm = pl.BlockSpec(memory_space=pl.ANY)
+    out = pl.pallas_call(
+        functools.partial(moe_kernel, nz),
+        out_shape=jax.ShapeDtypeStruct((count, width), bf16),
+        in_specs=[vmem] * 4 + [hbm] * 3,
+        out_specs=vmem,
+        scratch_shapes=[
+            pltpu.VMEM((nz, count, width + LANES), bf16),
+            pltpu.VMEM((2, width, hidden), bf16),
+            pltpu.VMEM((2, width, hidden), bf16),
+            pltpu.VMEM((2, hidden, width), bf16),
+            pltpu.VMEM(block, bf16),
+            pltpu.VMEM(block, bf16),
+            pltpu.VMEM(block, bf16),
+            pltpu.VMEM(block, bf16),
+            pltpu.VMEM((count, width), bf16),
+        ]
+        + [dma((3,))] * 3
+        + [dma((nz,))] * 8
+        + [dma(()), dma(())],
+        compiler_params=pltpu.CompilerParams(collective_id=0, has_side_effects=True),
+        name="moe",
+    )(tokens, norm_gain.reshape(1, width), routes, gate_scores, w_gate, w_up, w_down)
+    return out
+
+
+def body(tokens, norm_gain, routes, gate_scores, w_gate, w_up, w_down):
+    nexp = lax.axis_size("ep")
+    every_row = 2 * routes.shape[1] >= nexp
+    pairs = lax.axis_size("tp") == 2 and nexp % 2 == 0
+    one = exchange_body
+    if every_row and pairs and w_gate.shape[0] == 1 and 2 * nexp <= LANES:
+        one = gather_body
+    return one(tokens, norm_gain, routes, gate_scores, w_gate, w_up, w_down)
+
+
 def solution(mesh):
     in_specs = (
         P(("grp", "ep"), None),

time: 94.4 us -> 35.3 us (0.37)
  waiting for transfers between devices: 38.3 us -> 0 us
  Pallas kernels: 0 us -> 31.4 us
  blocking collectives: 27.4 us -> 0 us
  between operations: 13.5 us -> 0.01 us
  starting transfers between devices: 5.81 us -> 0 us
  matrix products: 3.4 us -> 0 us
  other arithmetic: 3.26 us -> 0 us
  local copies, waits for them, and re-layouts: 2.39 us -> 3.6 us
    pallas_call x0 -> x1, Pallas kernels: none -> 31.4 us  [gather_body(): pl.pallas_call(functools.partial(moe_kernel, nz), out_shape=jax.ShapeDtyp...]
    all_to_all x1 -> x0, blocking collectives: 27.4 us -> none  [body(): lax.all_to_all(outgoing, 'ep', split_axis=0, concat_axis=0, tiled=True)]
    all_to_all x1 -> x0, waiting for transfers between devices: 20.2 us -> none  [body(): lax.all_to_all(outputs.reshape(sources, places, outputs.shape[1]), 'ep',...]
    psum x1 -> x0, waiting for transfers between devices: 18.2 us -> none  [expert_rows(): total = lax.psum(part.astype(jnp.bfloat16), 'tp')]
    all_to_all x1 -> x0, starting transfers between devices: 5.81 us -> none  [body(): lax.all_to_all(outputs.reshape(sources, places, outputs.shape[1]), 'ep',...]
    dot_general x3 -> x0, matrix products: 3.4 us -> none  [the longest x1 1.94 us: expert_rows(): part = jnp.dot(act, wd, preferred_element_type=jnp.float32)]
    unnamed x10 -> x5, local copies, waits for them, and re-layouts: 0.83 us -> 3.6 us
    reduce_sum x4 -> x0, other arithmetic: 1.29 us -> none  [the longest x1 1.02 us: body(): jnp.mean(xf * xf, axis=-1, keepdims=True) + 1e-06]
  transfers between devices with their start and end apart: 2 -> 0, of which waited for: 2 -> 0; matrix products, arithmetic and copies ran while one was open for 0% -> 0% of each run, Pallas kernels for 0% -> 0%
where the time goes in v1:
time: 35.3 us; the launch traced here: 35.1 us
  Pallas kernels  31.4 us (89%)
  local copies, waits for them, and re-layouts  3.6 us (10%)
    pallas_call x1, Pallas kernels, gather_body(): pl.pallas_call(functools.partial(moe_kernel, nz), out_shape=jax.ShapeDtyp...  31.4 us
    unnamed x5, local copies, waits for them, and re-layouts  3.6 us

profile of v1, /device:TPU:0, one launch (start us, length us, event | category | flops | bytes accessed | tf_op | source)
XLA Modules:
  0.0 35.1 jit_solution(15883378838817720328)
XLA Ops:
  0.0 0.0 copy-start
  0.0 1.4 %copy.8.routes_ref = s32[24,4]{1,0:T(8,128)} copy(s32[24,4]{0,1:T(4,128)} %param.9) | data formatting | bytes 768 | tf_op args[2]
  1.4 0.0 copy-done
  1.4 0.7 %copy.9.score_ref = f32[24,4]{1,0:T(8,128)} copy(f32[24,4]{0,1:T(4,128)S(1)} %copy-done) | data formatting | bytes 768 | tf_op args[3]
  2.1 31.4 %moe.1 = bf16[24,2048]{1,0:T(8,128)(2,1)} custom-call(bf16[24,2048]{1,0:T(8,128)(2,1)} %tok_ref.1, f32[1,2048]{1,0:T(1,128)} %bitcast.1, s32[24,4]{1,0:T(8,128)} %copy.8.routes_ref, f32[24,4]{1,0:T(8,128)} %copy.9.score_ref, bf16[1,2048,256]{2,1,0:T(8,128)(2,1)} %wg_hbm.1, bf16[1,2048,256]{2,1,0:T(8,128)(2,1)} %wu_hbm.1, bf16[1,256,2048]{2,1,0:T(8,128)(2,1)} %wd_hbm.1), custom_call_target="tpu_custom_call" | custom-call | tf_op jit(solution)/shard_map/moe/pallas_call | solution.py:281
  33.5 1.5 %copy.11 = bf16[24,2048]{1,0:T(8,128)(2,1)} copy(bf16[24,2048]{1,0:T(8,128)(2,1)} %moe.1) | data formatting | bytes 196608
Async XLA Ops:
  0.0 1.4 %copy-start = (f32[24,4]{0,1:T(4,128)S(1)}, f32[24,4]{0,1:T(4,128)}, u32[]{:S(2)}) copy-start(f32[24,4]{0,1:T(4,128)} %param.10) | copy-start | bytes 1156

commit v2 on v1

--- a/solution.py
+++ b/solution.py
@@ -86,16 +86,16 @@
 
 def moe_kernel(
     nz,
-    tok_ref, gain_ref, routes_ref, score_ref, wg_hbm, wu_hbm, wd_hbm,
+    tok_hbm, gain_hbm, routes_hbm, score_hbm, wg_hbm, wu_hbm, wd_hbm,
     out_ref,
-    gath, wg, wu, wd, contrib, from_x, summed, from_z, res,
-    w_loc, w_send, w_recv, z_send, z_recv, x_send, x_recv,
+    tok_ref, gain_ref, routes_ref, score_ref, gath, wg, wu, wd, contrib, from_x, summed, from_z, res,
+    in_sem, w_loc, w_send, w_recv, z_send, z_recv, x_send, x_recv,
     rx_send, rx_recv, rz_send, rz_recv, f_send, f_recv,
 ):
     ep, tp = lax.axis_index("ep"), lax.axis_index("tp")
     z, x = ep // 2, ep % 2
     home = x == tp
-    count, width = tok_ref.shape
+    count, width = tok_hbm.shape
 
     def at_z(zz):
         return {"ep": zz * 2 + x, "tp": tp}
@@ -121,25 +121,30 @@
         )
         for i, (src, dst) in enumerate(weights)
     ]
-    for c in local:
+    inputs = [
+        pltpu.make_async_copy(src, dst, in_sem.at[i])
+        for i, (src, dst) in enumerate(
+            ((tok_hbm, tok_ref), (gain_hbm, gain_ref), (routes_hbm, routes_ref), (score_hbm, score_ref))
+        )
+    ]
+    for c in inputs + local:
         c.start()
+    for c in inputs:
+        c.wait()
 
     @pl.when(home)
     def _():
         xf = tok_ref[...].astype(jnp.float32)
         scale = lax.rsqrt(jnp.mean(xf * xf, axis=-1, keepdims=True) + 1e-06)
         gath[z, :, :width] = (xf * scale * gain_ref[...]).astype(jnp.bfloat16)
-        lane = lax.broadcasted_iota(jnp.int32, (count, LANES), 1)
+        line = lax.broadcasted_iota(jnp.int32, (LANES, count), 0)
         half = LANES // 2
-        expert = lane % half
-        w = jnp.zeros((count, LANES), jnp.float32)
-        for k in range(routes_ref.shape[1]):
-            w = w + jnp.where(routes_ref[:, k : k + 1] == expert, score_ref[:, k : k + 1], 0.0)
-        high = w.astype(jnp.bfloat16)
-        low = (w - high.astype(jnp.float32)).astype(jnp.bfloat16)
-        gath[z, :, width:] = jnp.where(
-            lane < half, high.astype(jnp.float32), low.astype(jnp.float32)
-        ).astype(jnp.bfloat16)
+        expert = line % half
+        w = jnp.zeros((LANES, count), jnp.float32)
+        for k in range(routes_ref.shape[0]):
+            w = w + jnp.where(routes_ref[k : k + 1, :] == expert, score_ref[k : k + 1, :], 0.0)
+        high = w.astype(jnp.bfloat16).astype(jnp.float32)
+        gath[z, :, width:] = jnp.where(line < half, high, w - high).T.astype(jnp.bfloat16)
 
     pl.semaphore_wait(barrier, nz + 1)
     for c in shared:
@@ -267,23 +272,29 @@
 
 
 ORDER = (1, 3, 2)
+VMEM_BYTES = 67043328
 
 
 def gather_body(tokens, norm_gain, routes, gate_scores, w_gate, w_up, w_down):
     count, width = tokens.shape
+    top = routes.shape[1]
     nz = lax.axis_size("ep") // 2
     hidden = w_gate.shape[2]
     bf16 = jnp.bfloat16
     dma = pltpu.SemaphoreType.DMA
     block = (nz, count, width)
     vmem = pl.BlockSpec(memory_space=pltpu.VMEM)
-    hbm = pl.BlockSpec(memory_space=pl.ANY)
+    hbm = pl.BlockSpec(memory_space=pltpu.HBM)
     out = pl.pallas_call(
         functools.partial(moe_kernel, nz),
         out_shape=jax.ShapeDtypeStruct((count, width), bf16),
-        in_specs=[vmem] * 4 + [hbm] * 3,
+        in_specs=[hbm] * 7,
         out_specs=vmem,
         scratch_shapes=[
+            pltpu.VMEM((count, width), bf16),
+            pltpu.VMEM((1, width), jnp.float32),
+            pltpu.VMEM((top, count), jnp.int32),
+            pltpu.VMEM((top, count), jnp.float32),
             pltpu.VMEM((nz, count, width + LANES), bf16),
             pltpu.VMEM((2, width, hidden), bf16),
             pltpu.VMEM((2, width, hidden), bf16),
@@ -294,12 +305,15 @@
             pltpu.VMEM(block, bf16),
             pltpu.VMEM((count, width), bf16),
         ]
+        + [dma((4,))]
         + [dma((3,))] * 3
         + [dma((nz,))] * 8
         + [dma(()), dma(())],
-        compiler_params=pltpu.CompilerParams(collective_id=0, has_side_effects=True),
+        compiler_params=pltpu.CompilerParams(
+            collective_id=0, has_side_effects=True, vmem_limit_bytes=VMEM_BYTES
+        ),
         name="moe",
-    )(tokens, norm_gain.reshape(1, width), routes, gate_scores, w_gate, w_up, w_down)
+    )(tokens, norm_gain.reshape(1, width), routes.T, gate_scores.T, w_gate, w_up, w_down)
     return out
 
 

time: 35.3 us -> 32.3 us (0.915)
  local copies, waits for them, and re-layouts: 3.6 us -> 1.54 us
  Pallas kernels: 31.4 us -> 30.6 us
    unnamed x5 -> x1, local copies, waits for them, and re-layouts: 3.6 us -> 1.54 us
    pallas_call x1, Pallas kernels: 31.4 us -> 30.6 us  [gather_body(): pl.pallas_call(functools.partial(moe_kernel, nz), out_shape=jax.ShapeDtyp...]
where the time goes in v2:
time: 32.3 us; the launch traced here: 32.2 us
  Pallas kernels  30.6 us (95%)
  local copies, waits for them, and re-layouts  1.54 us (5%)
    pallas_call x1, Pallas kernels, gather_body(): pl.pallas_call(functools.partial(moe_kernel, nz), out_shape=jax.ShapeDtyp...  30.6 us
    unnamed x1, local copies, waits for them, and re-layouts  1.54 us

profile of v2, /device:TPU:0, one launch (start us, length us, event | category | flops | bytes accessed | tf_op | source)
XLA Modules:
  0.0 32.2 jit_solution(7025128824013348320)
XLA Ops:
  0.0 30.6 %moe.1 = bf16[24,2048]{1,0:T(8,128)(2,1)} custom-call(bf16[24,2048]{1,0:T(8,128)(2,1)} %tok_hbm.1, f32[1,2048]{1,0:T(1,128)} %bitcast.3, s32[4,24]{1,0:T(4,128)} %bitcast.4, f32[4,24]{1,0:T(4,128)} %bitcast.5, bf16[1,2048,256]{2,1,0:T(8,128)(2,1)} %wg_hbm.1, bf16[1,2048,256]{2,1,0:T(8,128)(2,1)} %wu_hbm.1, bf16[1,256,2048]{2,1,0:T(8,128)(2,1)} %wd_hbm.1), custom_call_target="tpu_custom_call" | custom-call | tf_op jit(solution)/shard_map/moe/pallas_call | solution.py:288
  30.6 1.5 %copy.9 = bf16[24,2048]{1,0:T(8,128)(2,1)} copy(bf16[24,2048]{1,0:T(8,128)(2,1)} %moe.1) | data formatting | bytes 196608

commit v3 on v2

--- a/solution.py
+++ b/solution.py
@@ -84,6 +84,10 @@
     return finish(mixed)
 
 
+VMEM_BYTES = 66500000
+ROWS = 8
+
+
 def moe_kernel(
     nz,
     tok_hbm, gain_hbm, routes_hbm, score_hbm, wg_hbm, wu_hbm, wd_hbm,
@@ -102,7 +106,17 @@
 
     x_peer = {"ep": z * 2 + 1 - x, "tp": tp}
     sibling = {"ep": ep, "tp": 1 - tp}
-    others = [(z + k) % nz for k in range(1, nz)]
+    low = (z < nz // 2).astype(jnp.int32)
+
+    def far_first(k):
+        down = nz - 1 - k
+        down = down - (down <= z).astype(jnp.int32)
+        up = k + (k >= z).astype(jnp.int32)
+        return low * down + (1 - low) * up
+
+    others = [far_first(k) for k in range(nz - 1)]
+    order = [z] + others[::-1]
+    pieces = [pl.ds(r, ROWS) for r in range(0, count, ROWS)]
 
     barrier = pltpu.get_barrier_semaphore()
     for zz in others:
@@ -127,13 +141,15 @@
             ((tok_hbm, tok_ref), (gain_hbm, gain_ref), (routes_hbm, routes_ref), (score_hbm, score_ref))
         )
     ]
-    for c in inputs + local:
+    for c in local:
         c.start()
-    for c in inputs:
-        c.wait()
 
     @pl.when(home)
     def _():
+        for c in inputs:
+            c.start()
+        for c in inputs:
+            c.wait()
         xf = tok_ref[...].astype(jnp.float32)
         scale = lax.rsqrt(jnp.mean(xf * xf, axis=-1, keepdims=True) + 1e-06)
         gath[z, :, :width] = (xf * scale * gain_ref[...]).astype(jnp.bfloat16)
@@ -150,36 +166,19 @@
     for c in shared:
         c.start()
 
-    def along_z(zz, slot):
-        return pltpu.make_async_remote_copy(
-            gath.at[slot], gath.at[slot], z_send.at[zz], z_recv.at[slot],
+    def along_z(zz, slot, c):
+        part = gath.at[slot, pieces[c]]
+        return pltpu.make_async_remote_copy(
+            part, part, z_send.at[zz, c], z_recv.at[slot, c],
             device_id=at_z(zz), device_id_type=MESH,
         )
 
-    def across_x(slot):
-        return pltpu.make_async_remote_copy(
-            gath.at[slot], gath.at[slot], x_send.at[slot], x_recv.at[slot],
+    def across_x(slot, c):
+        part = gath.at[slot, pieces[c]]
+        return pltpu.make_async_remote_copy(
+            part, part, x_send.at[slot, c], x_recv.at[slot, c],
             device_id=x_peer, device_id_type=MESH,
         )
-
-    order = [z] + [(z + k) % nz for k in ORDER if k < nz]
-
-    @pl.when(home)
-    def _():
-        for zz in order[1:]:
-            along_z(zz, z).start()
-        across_x(z).start()
-
-    def arrive(slot, own):
-        @pl.when(home)
-        def _():
-            if not own:
-                along_z(slot, slot).wait_recv()
-                across_x(slot).start()
-
-        @pl.when(jnp.logical_not(home))
-        def _():
-            across_x(slot).wait_recv()
 
     def compute(slots):
         rows = jnp.concatenate(
@@ -209,70 +208,104 @@
                     y[i * count : (i + 1) * count] * weight[i]
                 ).astype(jnp.bfloat16)
 
-    def back_x(slot):
-        return pltpu.make_async_remote_copy(
-            contrib.at[slot], from_x.at[slot], rx_send.at[slot], rx_recv.at[slot],
+    def back_x(slot, c):
+        return pltpu.make_async_remote_copy(
+            contrib.at[slot, pieces[c]], from_x.at[slot, pieces[c]],
+            rx_send.at[slot, c], rx_recv.at[slot, c],
             device_id=x_peer, device_id_type=MESH,
         )
 
-    def back_z(zz, slot):
-        return pltpu.make_async_remote_copy(
-            summed.at[zz], from_z.at[slot], rz_send.at[zz], rz_recv.at[slot],
+    def back_z(zz, slot, c):
+        return pltpu.make_async_remote_copy(
+            summed.at[zz, pieces[c]], from_z.at[slot, pieces[c]],
+            rz_send.at[zz, c], rz_recv.at[slot, c],
             device_id=at_z(zz), device_id_type=MESH,
         )
 
-    for i, slot in enumerate(order):
-        arrive(slot, i == 0)
-    for c in local:
-        c.wait()
-    for c in shared:
-        c.wait()
-    compute(order)
-
-    back = order[1:] + order[:1]
+    def final(c):
+        part = res.at[pieces[c]]
+        return pltpu.make_async_remote_copy(
+            part, part, f_send.at[c], f_recv.at[c], device_id=sibling, device_id_type=MESH
+        )
+
+    def weights_here():
+        for c in local:
+            c.wait()
+        for c in shared:
+            c.wait()
+
+    parts = range(len(pieces))
+    cut = nz - 1
+    early, late = order[:cut], order[cut:]
+    back = early[1:][::-1] + late
+
+    def pair_sum(slot, c):
+        return contrib[slot, pieces[c]].astype(jnp.float32) + from_x[slot, pieces[c]].astype(
+            jnp.float32
+        )
+
+    @pl.when(home)
+    def _():
+        for zz in others:
+            for c in parts:
+                along_z(zz, z, c).start()
+        for c in parts:
+            across_x(z, c).start()
+        for slot in order[1:]:
+            for c in parts:
+                along_z(slot, slot, c).wait_recv()
+                across_x(slot, c).start()
+        weights_here()
+        compute(order)
+        for slot in back:
+            for c in parts:
+                back_x(slot, c).wait_recv()
+                summed[slot, pieces[c]] = pair_sum(slot, c).astype(jnp.bfloat16)
+                back_z(slot, z, c).start()
+        for c in parts:
+            back_x(z, c).wait_recv()
+        for c in parts:
+            total = pair_sum(z, c)
+            for slot in order[1:]:
+                back_z(slot, slot, c).wait_recv()
+                total = total + from_z[slot, pieces[c]].astype(jnp.float32)
+            res[pieces[c]] = total.astype(jnp.bfloat16)
+            final(c).start()
+            out_ref[pieces[c]] = total.astype(out_ref.dtype)
+        for c in parts:
+            for zz in others:
+                along_z(zz, z, c).wait_send()
+                back_z(zz, z, c).wait_send()
+            for slot in order:
+                across_x(slot, c).wait_send()
+            final(c).wait_send()
 
     @pl.when(jnp.logical_not(home))
     def _():
-        for slot in back:
-            back_x(slot).start()
-
-    final = pltpu.make_async_remote_copy(
-        res, res, f_send, f_recv, device_id=sibling, device_id_type=MESH
-    )
-
-    @pl.when(home)
-    def _():
-        for slot in back[:-1]:
-            back_x(slot).wait_recv()
-            summed[slot] = (
-                contrib[slot].astype(jnp.float32) + from_x[slot].astype(jnp.float32)
-            ).astype(jnp.bfloat16)
-            back_z(slot, z).start()
-        back_x(z).wait_recv()
-        total = contrib[z].astype(jnp.float32) + from_x[z].astype(jnp.float32)
-        for slot in back[:-1]:
-            back_z(slot, slot).wait_recv()
-            total = total + from_z[slot].astype(jnp.float32)
-        res[...] = total.astype(jnp.bfloat16)
-        final.start()
-        out_ref[...] = total.astype(out_ref.dtype)
-        for zz in order[1:]:
-            along_z(zz, z).wait_send()
-            back_z(zz, z).wait_send()
-        for slot in order:
-            across_x(slot).wait_send()
-        final.wait_send()
-
-    @pl.when(jnp.logical_not(home))
-    def _():
-        for slot in order:
-            back_x(slot).wait_send()
-        final.wait_recv()
-        out_ref[...] = res[...].astype(out_ref.dtype)
-
-
-ORDER = (1, 3, 2)
-VMEM_BYTES = 67043328
+        def take(slots):
+            for slot in slots:
+                for c in parts:
+                    across_x(slot, c).wait_recv()
+
+        def give(slots):
+            for slot in slots:
+                for c in parts:
+                    back_x(slot, c).start()
+
+        take(early)
+        weights_here()
+        compute(early)
+        give(early[1:][::-1])
+        take(late)
+        compute(late)
+        give(late)
+        give(early[:1])
+        for c in parts:
+            for slot in order:
+                back_x(slot, c).wait_send()
+        for c in parts:
+            final(c).wait_recv()
+            out_ref[pieces[c]] = res[pieces[c]].astype(out_ref.dtype)
 
 
 def gather_body(tokens, norm_gain, routes, gate_scores, w_gate, w_up, w_down):
@@ -287,7 +320,7 @@
     hbm = pl.BlockSpec(memory_space=pltpu.HBM)
     out = pl.pallas_call(
         functools.partial(moe_kernel, nz),
-        out_shape=jax.ShapeDtypeStruct((count, width), bf16),
+        out_shape=pltpu.VMEM((count, width), bf16),
         in_specs=[hbm] * 7,
         out_specs=vmem,
         scratch_shapes=[
@@ -307,8 +340,8 @@
         ]
         + [dma((4,))]
         + [dma((3,))] * 3
-        + [dma((nz,))] * 8
-        + [dma(()), dma(())],
+        + [dma((nz, count // ROWS))] * 8
+        + [dma((count // ROWS,))] * 2,
         compiler_params=pltpu.CompilerParams(
             collective_id=0, has_side_effects=True, vmem_limit_bytes=VMEM_BYTES
         ),
@@ -322,7 +355,8 @@
     every_row = 2 * routes.shape[1] >= nexp
     pairs = lax.axis_size("tp") == 2 and nexp % 2 == 0
     one = exchange_body
-    if every_row and pairs and w_gate.shape[0] == 1 and 2 * nexp <= LANES:
+    whole_rows = tokens.shape[0] % ROWS == 0
+    if whole_rows and every_row and pairs and w_gate.shape[0] == 1 and 2 * nexp <= LANES:
         one = gather_body
     return one(tokens, norm_gain, routes, gate_scores, w_gate, w_up, w_down)
 

time: 32.3 us -> 29.1 us (0.901)
  Pallas kernels: 30.6 us -> 28.3 us
  local copies, waits for them, and re-layouts: 1.54 us -> 0.64 us
    pallas_call x1, Pallas kernels: 30.6 us -> 28.3 us  [gather_body(): pl.pallas_call(functools.partial(moe_kernel, nz), out_shape=pltpu.VMEM((c...]
    unnamed x1, local copies, waits for them, and re-layouts: 1.54 us -> 0.64 us
where the time goes in v3:
time: 29.1 us; the launch traced here: 28.9 us
  Pallas kernels  28.3 us (97%)
  local copies, waits for them, and re-layouts  0.64 us (2%)
    pallas_call x1, Pallas kernels, gather_body(): pl.pallas_call(functools.partial(moe_kernel, nz), out_shape=pltpu.VMEM((c...  28.3 us
    unnamed x1, local copies, waits for them, and re-layouts  0.64 us

profile of v3, /device:TPU:0, one launch (start us, length us, event | category | flops | bytes accessed | tf_op | source)
XLA Modules:
  0.0 28.9 jit_solution(7792459259356322132)
XLA Ops:
  0.0 28.3 %moe.1 = bf16[24,2048]{1,0:T(8,128)(2,1)S(1)} custom-call(bf16[24,2048]{1,0:T(8,128)(2,1)} %tok_hbm.1, f32[1,2048]{1,0:T(1,128)} %bitcast.3, s32[4,24]{1,0:T(4,128)} %bitcast.4, f32[4,24]{1,0:T(4,128)} %bitcast.5, bf16[1,2048,256]{2,1,0:T(8,128)(2,1)} %wg_hbm.1, bf16[1,2048,256]{2,1,0:T(8,128)(2,1)} %wu_hbm.1, bf16[1,256,2048]{2,1,0:T(8,128)(2,1)} %wd_hbm.1), custom_call_target="tpu_custom_call" | custom-call | tf_op jit(solution)/shard_map/moe/pallas_call | solution.py:321
  28.3 0.6 %copy.9 = bf16[24,2048]{1,0:T(8,128)(2,1)} copy(bf16[24,2048]{1,0:T(8,128)(2,1)S(1)} %moe.1) | data formatting | bytes 196608

commit v4 on v3

--- a/solution.py
+++ b/solution.py
@@ -92,9 +92,9 @@
     nz,
     tok_hbm, gain_hbm, routes_hbm, score_hbm, wg_hbm, wu_hbm, wd_hbm,
     out_ref,
-    tok_ref, gain_ref, routes_ref, score_ref, gath, wg, wu, wd, contrib, from_x, summed, from_z, res,
+    tok_ref, gain_ref, routes_ref, score_ref, gath, wg, wu, wd, contrib, from_x, summed, from_z, from_far, res,
     in_sem, w_loc, w_send, w_recv, z_send, z_recv, x_send, x_recv,
-    rx_send, rx_recv, rz_send, rz_recv, f_send, f_recv,
+    rx_send, rx_recv, rz_send, rz_recv, far_send, far_recv, f_send, f_recv,
 ):
     ep, tp = lax.axis_index("ep"), lax.axis_index("tp")
     z, x = ep // 2, ep % 2
@@ -106,22 +106,17 @@
 
     x_peer = {"ep": z * 2 + 1 - x, "tp": tp}
     sibling = {"ep": ep, "tp": 1 - tp}
-    low = (z < nz // 2).astype(jnp.int32)
-
-    def far_first(k):
-        down = nz - 1 - k
-        down = down - (down <= z).astype(jnp.int32)
-        up = k + (k >= z).astype(jnp.int32)
-        return low * down + (1 - low) * up
-
-    others = [far_first(k) for k in range(nz - 1)]
-    order = [z] + others[::-1]
+    opposite = (z + nz // 2) % nz
+    others = [(z + k) % nz for k in range(1, nz) if k != nz // 2] + [opposite]
+    order = [z] + others
+    x_opposite = {"ep": opposite * 2 + 1 - x, "tp": tp}
     pieces = [pl.ds(r, ROWS) for r in range(0, count, ROWS)]
 
     barrier = pltpu.get_barrier_semaphore()
     for zz in others:
         pl.semaphore_signal(barrier, inc=1, device_id=at_z(zz), device_id_type=MESH)
     pl.semaphore_signal(barrier, inc=1, device_id=x_peer, device_id_type=MESH)
+    pl.semaphore_signal(barrier, inc=1, device_id=x_opposite, device_id_type=MESH)
     pl.semaphore_signal(barrier, inc=1, device_id=sibling, device_id_type=MESH)
 
     weights = ((wg_hbm, wg), (wu_hbm, wu), (wd_hbm, wd))
@@ -162,7 +157,7 @@
         high = w.astype(jnp.bfloat16).astype(jnp.float32)
         gath[z, :, width:] = jnp.where(line < half, high, w - high).T.astype(jnp.bfloat16)
 
-    pl.semaphore_wait(barrier, nz + 1)
+    pl.semaphore_wait(barrier, nz + 2)
     for c in shared:
         c.start()
 
@@ -215,9 +210,15 @@
             device_id=x_peer, device_id_type=MESH,
         )
 
-    def back_z(zz, slot, c):
-        return pltpu.make_async_remote_copy(
-            summed.at[zz, pieces[c]], from_z.at[slot, pieces[c]],
+    def straight(slot, c):
+        return pltpu.make_async_remote_copy(
+            contrib.at[slot, pieces[c]], from_far.at[pieces[c]], far_send.at[c], far_recv.at[c],
+            device_id=x_opposite, device_id_type=MESH,
+        )
+
+    def back_z(zz, slot, c, source=summed):
+        return pltpu.make_async_remote_copy(
+            source.at[zz, pieces[c]], from_z.at[slot, pieces[c]],
             rz_send.at[zz, c], rz_recv.at[slot, c],
             device_id=at_z(zz), device_id_type=MESH,
         )
@@ -235,9 +236,7 @@
             c.wait()
 
     parts = range(len(pieces))
-    cut = nz - 1
-    early, late = order[:cut], order[cut:]
-    back = early[1:][::-1] + late
+    early = order[:-1]
 
     def pair_sum(slot, c):
         return contrib[slot, pieces[c]].astype(jnp.float32) + from_x[slot, pieces[c]].astype(
@@ -257,7 +256,9 @@
                 across_x(slot, c).start()
         weights_here()
         compute(order)
-        for slot in back:
+        for c in parts:
+            back_z(opposite, z, c, contrib).start()
+        for slot in early[1:]:
             for c in parts:
                 back_x(slot, c).wait_recv()
                 summed[slot, pieces[c]] = pair_sum(slot, c).astype(jnp.bfloat16)
@@ -266,6 +267,8 @@
             back_x(z, c).wait_recv()
         for c in parts:
             total = pair_sum(z, c)
+            straight(z, c).wait_recv()
+            total = total + from_far[pieces[c]].astype(jnp.float32)
             for slot in order[1:]:
                 back_z(slot, slot, c).wait_recv()
                 total = total + from_z[slot, pieces[c]].astype(jnp.float32)
@@ -292,16 +295,23 @@
                 for c in parts:
                     back_x(slot, c).start()
 
-        take(early)
-        weights_here()
-        compute(early)
-        give(early[1:][::-1])
-        take(late)
-        compute(late)
-        give(late)
-        give(early[:1])
-        for c in parts:
-            for slot in order:
+        done = 0
+        for size in (nz - 2, 1, 1):
+            slots = order[done : done + size]
+            done += size
+            take(slots)
+            if size == done:
+                weights_here()
+            compute(slots)
+            if slots[-1] is opposite:
+                for c in parts:
+                    straight(opposite, c).start()
+            give([s for s in slots if s is not z and s is not opposite])
+        give([z])
+        for c in parts:
+            straight(opposite, c).wait_send()
+        for c in parts:
+            for slot in early:
                 back_x(slot, c).wait_send()
         for c in parts:
             final(c).wait_recv()
@@ -337,11 +347,12 @@
             pltpu.VMEM(block, bf16),
             pltpu.VMEM(block, bf16),
             pltpu.VMEM((count, width), bf16),
+            pltpu.VMEM((count, width), bf16),
         ]
         + [dma((4,))]
         + [dma((3,))] * 3
         + [dma((nz, count // ROWS))] * 8
-        + [dma((count // ROWS,))] * 2,
+        + [dma((count // ROWS,))] * 4,
         compiler_params=pltpu.CompilerParams(
             collective_id=0, has_side_effects=True, vmem_limit_bytes=VMEM_BYTES
         ),
@@ -353,7 +364,7 @@
 def body(tokens, norm_gain, routes, gate_scores, w_gate, w_up, w_down):
     nexp = lax.axis_size("ep")
     every_row = 2 * routes.shape[1] >= nexp
-    pairs = lax.axis_size("tp") == 2 and nexp % 2 == 0
+    pairs = lax.axis_size("tp") == 2 and nexp % 4 == 0 and nexp >= 8
     one = exchange_body
     whole_rows = tokens.shape[0] % ROWS == 0
     if whole_rows and every_row and pairs and w_gate.shape[0] == 1 and 2 * nexp <= LANES:

time: 29.1 us -> 27.3 us (0.938)
  Pallas kernels: 28.3 us -> 26.5 us
    pallas_call x1, Pallas kernels: 28.3 us -> 26.5 us  [gather_body(): pl.pallas_call(functools.partial(moe_kernel, nz), out_shape=pltpu.VMEM((c...]
where the time goes in v4:
time: 27.3 us; the launch traced here: 27.1 us
  Pallas kernels  26.5 us (97%)
  local copies, waits for them, and re-layouts  0.64 us (2%)
    pallas_call x1, Pallas kernels, gather_body(): pl.pallas_call(functools.partial(moe_kernel, nz), out_shape=pltpu.VMEM((c...  26.5 us
    unnamed x1, local copies, waits for them, and re-layouts  0.64 us

profile of v4, /device:TPU:0, one launch (start us, length us, event | category | flops | bytes accessed | tf_op | source)
XLA Modules:
  0.0 27.1 jit_solution(8284633112936810306)
XLA Ops:
  0.0 26.5 %moe.1 = bf16[24,2048]{1,0:T(8,128)(2,1)S(1)} custom-call(bf16[24,2048]{1,0:T(8,128)(2,1)} %tok_hbm.1, f32[1,2048]{1,0:T(1,128)} %bitcast.3, s32[4,24]{1,0:T(4,128)} %bitcast.4, f32[4,24]{1,0:T(4,128)} %bitcast.5, bf16[1,2048,256]{2,1,0:T(8,128)(2,1)} %wg_hbm.1, bf16[1,2048,256]{2,1,0:T(8,128)(2,1)} %wu_hbm.1, bf16[1,256,2048]{2,1,0:T(8,128)(2,1)} %wd_hbm.1), custom_call_target="tpu_custom_call" | custom-call | tf_op jit(solution)/shard_map/moe/pallas_call | solution.py:331
  26.5 0.6 %copy.9 = bf16[24,2048]{1,0:T(8,128)(2,1)} copy(bf16[24,2048]{1,0:T(8,128)(2,1)S(1)} %moe.1) | data formatting | bytes 196608

commit v5 on v4

--- a/solution.py
+++ b/solution.py
@@ -307,7 +307,8 @@
                 for c in parts:
                     straight(opposite, c).start()
             give([s for s in slots if s is not z and s is not opposite])
-        give([z])
+            if done == nz - 1:
+                give([z])
         for c in parts:
             straight(opposite, c).wait_send()
         for c in parts:

time: 27.3 us -> 26.7 us (0.978)
  Pallas kernels: 26.5 us -> 25.9 us
    pallas_call x1, Pallas kernels: 26.5 us -> 25.9 us  [gather_body(): pl.pallas_call(functools.partial(moe_kernel, nz), out_shape=pltpu.VMEM((c...]
where the time goes in v5:
time: 26.7 us; the launch traced here: 26.6 us
  Pallas kernels  25.9 us (97%)
  local copies, waits for them, and re-layouts  0.64 us (2%)
    pallas_call x1, Pallas kernels, gather_body(): pl.pallas_call(functools.partial(moe_kernel, nz), out_shape=pltpu.VMEM((c...  25.9 us
    unnamed x1, local copies, waits for them, and re-layouts  0.64 us

profile of v5, /device:TPU:0, one launch (start us, length us, event | category | flops | bytes accessed | tf_op | source)
XLA Modules:
  0.0 26.6 jit_solution(11552579737455801407)
XLA Ops:
  0.0 25.9 %moe.1 = bf16[24,2048]{1,0:T(8,128)(2,1)S(1)} custom-call(bf16[24,2048]{1,0:T(8,128)(2,1)} %tok_hbm.1, f32[1,2048]{1,0:T(1,128)} %bitcast.3, s32[4,24]{1,0:T(4,128)} %bitcast.4, f32[4,24]{1,0:T(4,128)} %bitcast.5, bf16[1,2048,256]{2,1,0:T(8,128)(2,1)} %wg_hbm.1, bf16[1,2048,256]{2,1,0:T(8,128)(2,1)} %wu_hbm.1, bf16[1,256,2048]{2,1,0:T(8,128)(2,1)} %wd_hbm.1), custom_call_target="tpu_custom_call" | custom-call | tf_op jit(solution)/shard_map/moe/pallas_call | solution.py:332
  26.0 0.6 %copy.9 = bf16[24,2048]{1,0:T(8,128)(2,1)} copy(bf16[24,2048]{1,0:T(8,128)(2,1)S(1)} %moe.1) | data formatting | bytes 196608
